TPU v7x, 32 devices: a whole 2x2x4 slice. The times are simulated.
32 devices in a mesh: fs: 8 (over z, y), tp: 4 (over x, core).
Axes of the slice: x: 2, y: 2, z: 4, core: 2. Of those that a mesh axis runs over, the one named last changes fastest.
Arguments:
- inputs: bfloat16 [9216, 2048], P('fs'), may hold values from -6 to 6
- gate_cot: bfloat16 [9216, 4096], P('fs', 'tp'), may hold values from -0.0546875 to 0.0546875
- state_cot: bfloat16 [9216, 1024], P('fs', 'tp'), may hold values from -0.0546875 to 0.0546875
- gate_weight: float32 [2048, 4096], P('fs', 'tp'), may hold values from -0.75 to 0.75
- state_weight: float32 [2048, 1024], P('fs', 'tp'), may hold values from -0.75 to 0.75
- gate_factor: bfloat16 [2048, 256], P('fs'), may hold values from -0.375 to 0.375
- state_factor: bfloat16 [2048, 256], P('fs'), may hold values from -0.375 to 0.375
- gate_first: float32 [256, 4096], P('fs', 'tp'), may hold values from -6 to 6
- gate_second: float32 [256, 4096], P('fs', 'tp'), may hold values from 0.3 to 3
- state_first: float32 [256, 1024], P('fs', 'tp'), may hold values from -6 to 6
- state_second: float32 [256, 1024], P('fs', 'tp'), may hold values from 0.3 to 3
Outputs:
- new_gate_weight: float32 [2048, 4096], P('fs', 'tp')
- new_state_weight: float32 [2048, 1024], P('fs', 'tp')
- gate_copy: bfloat16 [2048, 4096], P(None, 'tp')
- state_copy: bfloat16 [2048, 1024], P(None, 'tp')
- new_gate_first: float32 [256, 4096], P('fs', 'tp')
- new_gate_second: float32 [256, 4096], P('fs', 'tp')
- new_state_first: float32 [256, 1024], P('fs', 'tp')
- new_state_second: float32 [256, 1024], P('fs', 'tp')
All inputs are finite; a program needn't handle non-finite values.
Results may differ from a plain program's by a relative error of at most 0.004.
Values may be sent and summed in bfloat16 or wider, within the bound.
A program may use at most 128 MiB of HBM per device.

v0:
```python
import functools

import jax
import jax.numpy as jnp
from jax import lax
from jax.experimental import pallas as pl
from jax.experimental.pallas import tpu as pltpu
from jax.sharding import PartitionSpec as P

MESH = pl.DeviceIdType.MESH
BF16 = jnp.bfloat16
F32 = jnp.float32


def over_rows(a, b):
    return lax.dot_general(a, b, (((0,), (0,)), ((), ())), preferred_element_type=F32)


def split(a):
    upper = a.astype(BF16)
    return upper, (a - upper.astype(F32)).astype(BF16)


def exchange_kernel(
    n, tp, tiles,
    x_hbm, gcot_hbm, scot_hbm, gw_hbm, sw_hbm, gf_hbm, sf_hbm, gfirst_hbm, gsecond_hbm, sfirst_hbm, ssecond_hbm,
    wg, f_all, dirs, sums_all, fnew, snew,
    x, gcot, scot, wide, wown, first, second, acc, send_y, recv_y, send_z, recv_z, sums, sums_in,
    load, store,
    f_send, f_recv, fx_send, fx_recv, fc_send, fc_recv, fd_send, fd_recv,
    ry_send, ry_recv, rz_send, rz_recv, d_send, d_recv, s_send, s_recv, w_send, w_recv,
):
    me = lax.axis_index("fs")
    t = lax.axis_index("tp")
    rows, rank = gf_hbm.shape
    gc = gcot.shape[1]
    sc = scot.shape[1]
    r = first.shape[0]
    q = rows // tp
    half = rows // 2
    depth = n // 2
    z, y = me // 2, me % 2
    partner = 2 * z + 1 - y

    sources = [
        (gf_hbm, f_all.at[me, :, pl.ds(0, rank)]),
        (sf_hbm, f_all.at[me, :, pl.ds(rank, rank)]),
        (gw_hbm, wide.at[:, pl.ds(0, gc)]),
        (sw_hbm, wide.at[:, pl.ds(gc, sc)]),
        (x_hbm, x),
        (gcot_hbm, gcot),
        (scot_hbm, scot),
        (gfirst_hbm, first.at[:, pl.ds(0, gc)]),
        (sfirst_hbm, first.at[:, pl.ds(gc, sc)]),
        (gsecond_hbm, second.at[:, pl.ds(0, gc)]),
        (ssecond_hbm, second.at[:, pl.ds(gc, sc)]),
    ]
    loads = [pltpu.make_async_copy(src, dst, load.at[k]) for k, (src, dst) in enumerate(sources)]
    for c in loads:
        c.start()

    def along_z(k):
        return 2 * ((z + depth + k) % depth) + y

    barrier = pltpu.get_barrier_semaphore()
    pl.semaphore_signal(barrier, inc=1, device_id=(partner, t), device_id_type=MESH)
    for k in range(1, depth):
        pl.semaphore_signal(barrier, inc=1, device_id=(along_z(k), t), device_id_type=MESH)
    for d in range(1, tp):
        pl.semaphore_signal(barrier, inc=1, device_id=(me, (t + d) % tp), device_id_type=MESH)
    pl.semaphore_wait(barrier, depth + tp - 1)

    def remote(src, dst, ss, rs, dev):
        return pltpu.make_async_remote_copy(
            src_ref=src, dst_ref=dst, send_sem=ss, recv_sem=rs, device_id=dev, device_id_type=MESH
        )

    core_peer = t + 1 - 2 * (t % 2)
    x_peer = (t + 2) % tp

    def source_block(j):
        k = j % depth
        return 2 * ((z + depth - k) % depth) + (y if j < depth else 1 - y)

    def quarter(block, which):
        return f_all.at[block, pl.ds(which * q, q), :]

    def first_leg(view, send, recv):
        copies = {}
        for j in sorted(range(1, depth), key=lambda k: -min(k, depth - k)) + [depth]:
            dev = partner if j == depth else along_z(j)
            copies[j] = remote(view(me), view(me), send.at[j], recv.at[j], (dev, t))
            copies[j].start()
        return copies

    def pass_over(copies, view, send, recv, k):
        b = source_block(k)
        copies[depth + k] = remote(
            view(b), view(b), send.at[depth + k], recv.at[depth + k], (partner, t)
        )
        copies[depth + k].start()

    loads[0].wait()
    loads[1].wait()
    mine = lambda b: quarter(b, t)
    f_copies = first_leg(mine, f_send, f_recv)

    loads[2].wait()
    loads[3].wait()
    wown[...] = wide[...].astype(BF16)

    shares = {}

    def share(j):
        src = quarter(source_block(j), t)
        cx = remote(src, src, fx_send.at[j], fx_recv.at[j], (me, x_peer))
        cx.start()
        cc = remote(src, src, fc_send.at[j], fc_recv.at[j], (me, core_peer))
        cc.start()
        shares[j] = [cx, cc]

    order = sorted(range(1, depth), key=lambda k: min(k, depth - k))
    for k in order:
        f_copies[k].wait_recv()
        pass_over(f_copies, mine, f_send, f_recv, k)
        share(k)

    pos = z + y * (n - 1 - 2 * z)

    def at_pos(p):
        p = (p + n) % n
        far = p // (n // 2)
        return 2 * p * (1 - far) + far * (2 * (n - 1 - p) + 1)

    right, left = at_pos(pos + 1), at_pos(pos - 1)
    steps = n // 2

    def w_copy(way, s, h):
        block = at_pos(pos - s) if way == 0 else at_pos(pos + s)
        dst = wg.at[block, pl.ds(h * half, half), :]
        src = wown.at[pl.ds(h * half, half), :] if s == 0 else dst
        return remote(
            src, dst, w_send.at[way, s, h], w_recv.at[way, s, h], (right if way == 0 else left, t)
        )

    def halves(way, s):
        return (0, 1) if s < steps - 1 else (way,)

    w_copies = {}

    def ring_step(s, parts=(0, 1)):
        for k in parts:
            for way in (0, 1):
                h = k if way == 0 else 1 - k
                if s > 0:
                    w_copies[way, s - 1, h].wait_recv()
                if h in halves(way, s):
                    w_copies[way, s, h] = w_copy(way, s, h)
                    w_copies[way, s, h].start()

    ring_step(0)
    own_w = pltpu.make_async_copy(wown, wg.at[me], store.at[0])
    own_w.start()

    for k in [0] + order:
        f_copies[depth + k].wait_recv()
        share(depth + k)
    for j, pair in shares.items():
        pair[0].wait_recv()
        src = quarter(source_block(j), x_peer)
        cd = remote(src, src, fd_send.at[j], fd_recv.at[j], (me, core_peer))
        cd.start()
        pair.append(cd)
    for cx, cc, cd in shares.values():
        cc.wait_recv()
        cd.wait_recv()

    ring_step(1, (0,))
    for k in (4, 5, 6):
        loads[k].wait()
    factor = f_all.reshape(n * rows, 2 * rank)
    step = x.shape[0] // tiles
    acc[...] = jnp.zeros_like(acc)

    def tile(i, carry):
        at = pl.ds(pl.multiple_of(i * step, step), step)
        upper, lower = split(jnp.dot(x[at, :], factor[...], preferred_element_type=F32))
        g, s = gcot[at, :], scot[at, :]
        acc[:, :gc] += over_rows(upper[:, :rank], g) + over_rows(lower[:, :rank], g)
        acc[:, gc:] += over_rows(upper[:, rank:], s) + over_rows(lower[:, rank:], s)
        return carry

    lax.fori_loop(0, tiles, tile, 0)

    def part_of(block):
        return acc[pl.ds(pl.multiple_of(block * r, r), r), :]

    out_order = list(range(1, depth)) + [0]
    y_copies = {}
    for k in out_order:
        send_y[k] = part_of(2 * ((z + k) % depth) + 1 - y).astype(BF16)
        y_copies[k] = remote(send_y.at[k], recv_y.at[k], ry_send.at[k], ry_recv.at[k], (partner, t))
        y_copies[k].start()
    ring_step(1, (1,))

    grams = []
    for k in (0, 1):
        part = factor[:, k * rank:(k + 1) * rank]
        grams.append(split(over_rows(part, part)))

    z_copies = {}
    for k in range(1, depth):
        y_copies[k].wait_recv()
        send_z[k] = (part_of(along_z(k)) + recv_y[k].astype(F32)).astype(BF16)
        z_copies[k] = remote(send_z.at[k], recv_z.at[k], rz_send.at[k], rz_recv.at[k], (along_z(k), t))
        z_copies[k].start()

    ring_step(2, (0,))

    for c in loads[7:]:
        c.wait()
    y_copies[0].wait_recv()
    total = part_of(me) + recv_y[0].astype(F32)
    for k in range(1, depth):
        z_copies[k].wait_recv()
        total = total + recv_z[k].astype(F32)
    new_first = 0.8 * first[...] + 0.2 * total
    new_second = 0.9 * second[...] + 0.1 * total * total
    fnew[...] = new_first
    snew[...] = new_second
    dirs[me] = (new_first / jnp.sqrt(new_second)).astype(BF16)
    view = lambda b: dirs.at[b]
    d_copies = first_leg(view, d_send, d_recv)
    for k in order:
        d_copies[k].wait_recv()
        pass_over(d_copies, view, d_send, d_recv, k)

    ring_step(2, (1,))
    for k in range(depth):
        d_copies[depth + k].wait_recv()
    both = dirs[...].reshape(n * r, dirs.shape[2])
    squares = []
    for (upper, lower), part in zip(grams, (both[:, :gc], both[:, gc:])):
        lifted = jnp.dot(upper, part, preferred_element_type=F32)
        lifted = lifted + jnp.dot(lower, part, preferred_element_type=F32)
        squares.append(jnp.sum(part.astype(F32) * lifted))
    row = lax.broadcasted_iota(jnp.int32, sums.shape, 0)
    sums[...] = jnp.where(row == 0, squares[0], squares[1])
    s_copies = []
    for d in range(1, tp):
        c = remote(sums, sums_in.at[d], s_send.at[d], s_recv.at[d], (me, (t + d) % tp))
        c.start()
        s_copies.append(c)

    for s in range(3, steps):
        ring_step(s)
    for c in s_copies:
        c.wait()
    whole = sums[...]
    for d in range(1, tp):
        whole = whole + sums_in[d]
    sums_all[...] = whole
    for way in (0, 1):
        for h in halves(way, steps - 1):
            w_copies[way, steps - 1, h].wait_recv()
    for group in (w_copies, f_copies, y_copies, z_copies, d_copies):
        for c in group.values():
            c.wait_send()
    for trio in shares.values():
        for c in trio:
            c.wait_send()
    own_w.wait()


def finish_kernel(
    sizes, wg, f_blk, dirs, sums, gw, sw, gf, sf, fnew, snew,
    gcopy, scopy, gnew, snew_w, gf_out, gs_out, sf_out, ss_out,
):
    gc = gw.shape[1]
    rank = gf.shape[1]
    both = dirs[...].reshape(dirs.shape[0] * dirs.shape[1], dirs.shape[2])
    gdir, sdir = both[:, :gc], both[:, gc:]
    gscale = 0.02 / jnp.sqrt(sums[0:1, 0:1] / sizes[0] + 0.25)
    sscale = 0.02 / jnp.sqrt(sums[1:2, 0:1] / sizes[1] + 0.25)
    w = wg[0]
    f = f_blk[0]
    gfull = jnp.dot(f[:, :rank], gdir, preferred_element_type=F32)
    sfull = jnp.dot(f[:, rank:], sdir, preferred_element_type=F32)
    gcopy[...] = (w[:, :gc].astype(F32) - gscale * gfull).astype(BF16)
    scopy[...] = (w[:, gc:].astype(F32) - sscale * sfull).astype(BF16)

    @pl.when(pl.program_id(0) == 0)
    def _():
        gnew[...] = gw[...] - gscale * jnp.dot(gf[...], gdir, preferred_element_type=F32)
        snew_w[...] = sw[...] - sscale * jnp.dot(sf[...], sdir, preferred_element_type=F32)
        gf_out[...] = fnew[:, :gc]
        sf_out[...] = fnew[:, gc:]
        gs_out[...] = snew[:, :gc]
        ss_out[...] = snew[:, gc:]


def per_device(
    n, tp, inputs, gate_cot, state_cot, gate_weight, state_weight, gate_factor, state_factor,
    gate_first, gate_second, state_first, state_second,
):
    tokens, d = inputs.shape
    rows, gc = gate_weight.shape
    sc = state_weight.shape[1]
    cols = gc + sc
    rank = gate_factor.shape[1]
    r = gate_first.shape[0]
    tiles = 3 if tokens % (3 * 128) == 0 else 1
    dma = pltpu.SemaphoreType.DMA
    anys = pl.BlockSpec(memory_space=pl.ANY)
    sds = jax.ShapeDtypeStruct
    steps = n // 2
    wg, f_all, dirs, sums, fnew, snew = pl.pallas_call(
        functools.partial(exchange_kernel, n, tp, tiles),
        out_shape=(
            sds((n, rows, cols), BF16),
            sds((n, rows, 2 * rank), BF16),
            sds((n, r, cols), BF16),
            sds((8, 128), F32),
            sds((r, cols), F32),
            sds((r, cols), F32),
        ),
        in_specs=[anys] * 11,
        out_specs=[anys] + [pl.BlockSpec(memory_space=pltpu.VMEM)] * 5,
        scratch_shapes=[
            pltpu.VMEM((tokens, d), BF16),
            pltpu.VMEM((tokens, gc), BF16),
            pltpu.VMEM((tokens, sc), BF16),
            pltpu.VMEM((rows, cols), F32),
            pltpu.VMEM((rows, cols), BF16),
            pltpu.VMEM((r, cols), F32),
            pltpu.VMEM((r, cols), F32),
            pltpu.VMEM((rank, cols), F32),
        ]
        + [pltpu.VMEM((steps, r, cols), BF16)] * 4
        + [
            pltpu.VMEM((8, 128), F32),
            pltpu.VMEM((tp, 8, 128), F32),
            dma((11,)),
            dma((1,)),
        ]
        + [dma((n,))] * 8
        + [dma((steps,))] * 4
        + [dma((n,))] * 2
        + [dma((tp,))] * 2
        + [dma((2, steps, 2))] * 2,
        compiler_params=pltpu.CompilerParams(
            collective_id=0, has_side_effects=True, vmem_limit_bytes=60 * 1024 * 1024
        ),
        name="exchange",
    )(
        inputs, gate_cot, state_cot, gate_weight, state_weight, gate_factor, state_factor,
        gate_first, gate_second, state_first, state_second,
    )

    def whole(a):
        return pl.BlockSpec(a.shape, lambda b: (0,) * len(a.shape))

    sizes = (n * rows * gc * tp, n * rows * sc * tp)
    fixed = (gate_weight, state_weight, gate_factor, state_factor, fnew, snew)
    outs = (gate_weight, state_weight, gate_first, gate_second, state_first, state_second)
    gcopy, scopy, gnew, snew_w, *small = pl.pallas_call(
        functools.partial(finish_kernel, sizes),
        grid=(n,),
        out_shape=(sds((n * rows, gc), BF16), sds((n * rows, sc), BF16))
        + tuple(sds(a.shape, a.dtype) for a in outs),
        in_specs=[
            pl.BlockSpec((1, rows, cols), lambda b: (b, 0, 0)),
            pl.BlockSpec((1, rows, 2 * rank), lambda b: (b, 0, 0)),
            whole(dirs),
            whole(sums),
        ]
        + [whole(a) for a in fixed],
        out_specs=[
            pl.BlockSpec((rows, gc), lambda b: (b, 0)),
            pl.BlockSpec((rows, sc), lambda b: (b, 0)),
        ]
        + [whole(a) for a in outs],
        compiler_params=pltpu.CompilerParams(vmem_limit_bytes=58 * 1024 * 1024),
        name="finish",
    )(wg, f_all, dirs, sums, *fixed)
    return (gnew, snew_w, gcopy, scopy, *small)


def lifted_product(inputs, factor, cot):
    upper, lower = split(jnp.dot(inputs, factor, preferred_element_type=F32))
    first_part = jnp.einsum("tr,tc->rc", upper, cot, preferred_element_type=F32)
    return first_part + jnp.einsum("tr,tc->rc", lower, cot, preferred_element_type=F32)


def with_collectives(
    n, tp, inputs, gate_cot, state_cot, gate_weight, state_weight, gate_factor, state_factor,
    gate_first, gate_second, state_first, state_second,
):
    gc = gate_cot.shape[1]
    gate_part = lifted_product(inputs, lax.all_gather(gate_factor, "fs", axis=0, tiled=True), gate_cot)
    state_part = lifted_product(inputs, lax.all_gather(state_factor, "fs", axis=0, tiled=True), state_cot)
    partial_proj = jnp.concatenate([gate_part, state_part], 1)
    projection = lax.psum_scatter(partial_proj, "fs", scatter_dimension=0, tiled=True)
    first_new = 0.8 * jnp.concatenate([gate_first, state_first], 1) + 0.2 * projection
    second_new = 0.9 * jnp.concatenate([gate_second, state_second], 1) + 0.1 * projection * projection
    direction = (first_new / jnp.sqrt(second_new)).astype(BF16)
    dirs = lax.all_gather(direction, "fs", axis=0, tiled=True)
    gate_full = jnp.dot(gate_factor, dirs[:, :gc], preferred_element_type=F32)
    state_full = jnp.dot(state_factor, dirs[:, gc:], preferred_element_type=F32)
    gate_sq, state_sq = lax.psum(
        (jnp.sum(gate_full * gate_full), jnp.sum(state_full * state_full)), ("fs", "tp")
    )
    gate_scale = 0.02 / jnp.sqrt(gate_sq / (gate_full.size * n * tp) + 0.25)
    state_scale = 0.02 / jnp.sqrt(state_sq / (state_full.size * n * tp) + 0.25)
    gate_new = gate_weight - gate_scale * gate_full
    state_new = state_weight - state_scale * state_full
    gate_copy = lax.all_gather(gate_new.astype(BF16), "fs", axis=0, tiled=True)
    state_copy = lax.all_gather(state_new.astype(BF16), "fs", axis=0, tiled=True)
    return (
        gate_new, state_new, gate_copy, state_copy,
        first_new[:, :gc], second_new[:, :gc], first_new[:, gc:], second_new[:, gc:],
    )


def solution(mesh):
    n, tp = mesh.shape["fs"], mesh.shape["tp"]
    both = P("fs", "tp")
    wide = P("fs", None)

    def body(*args):
        r = args[7].shape[0]
        quarter = args[5].shape[0] // tp
        fits = tp == 4 and r % 16 == 0 and quarter % 16 == 0 and n >= 8
        return (per_device if fits else with_collectives)(n, tp, *args)

    return jax.shard_map(
        body,
        mesh=mesh,
        in_specs=(wide, both, both, both, both, wide, wide, both, both, both, both),
        out_specs=(both, both, P(None, "tp"), P(None, "tp"), both, both, both, both),
        check_vma=False,
    )
```

profile of v0, /device:TPU:0, one launch (start us, length us, event | category | flops | bytes accessed | tf_op | source)
XLA Modules:
  0.0 94.1 jit_solution(343314153815328242)
XLA Ops:
  0.6 83.0 %exchange.1 = (bf16[8,256,1280]{2,1,0:T(8,128)(2,1)}, bf16[8,256,512]{2,1,0:T(8,128)(2,1)}, bf16[8,32,1280]{2,1,0:T(8,128)(2,1)}, f32[8,128]{1,0:T(8,128)}, f32[32,1280]{1,0:T(8,128)}, /*index=5*/f32[32,1280]{1,0:T(8,128)}) custom-call(bf16[1152,2048]{1,0:T(8,128)(2,1)} %x_hbm.1, bf16[1152,1024]{1,0:T(8,128)(2,1)} %gcot_hbm.1, bf16[1152,256]{1,0:T(8,128)(2,1)} %scot_hbm.1, ...), custom_call_target="tpu_custom_call" | custom-call | tf_op jit(solution)/shard_map/exchange/pallas_call | solution.py:317
  83.7 10.4 %finish.1 = (bf16[2048,1024]{1,0:T(8,128)(2,1)}, bf16[2048,256]{1,0:T(8,128)(2,1)}, f32[256,1024]{1,0:T(8,128)}, f32[256,256]{1,0:T(8,128)}, f32[32,1024]{1,0:T(...) custom-call(bf16[8,256,1280]{2,1,0:T(8,128)(2,1)} %get-tuple-element.22.wg, ...), custom_call_target="tpu_custom_call" | custom-call | tf_op jit(solution)/shard_map/finish/pallas_call | solution.py:366
where the time goes:
time: 94.4 us; the launch traced here: 94.1 us
  Pallas kernels  93.4 us (99%)
    pallas_call x1, Pallas kernels, per_device(): pl.pallas_call(functools.partial(exchange_kernel, n, tp, tiles), out_shap...  83 us
    pallas_call x1, Pallas kernels, per_device(): pl.pallas_call(functools.partial(finish_kernel, sizes), grid=(n,), out_sh...  10.4 us

commit v1 on v0

--- a/solution.py
+++ b/solution.py
@@ -22,11 +22,11 @@
 
 
 def exchange_kernel(
-    n, tp, tiles,
+    n, tp, tiles, sizes,
     x_hbm, gcot_hbm, scot_hbm, gw_hbm, sw_hbm, gf_hbm, sf_hbm, gfirst_hbm, gsecond_hbm, sfirst_hbm, ssecond_hbm,
-    wg, f_all, dirs, sums_all, fnew, snew,
-    x, gcot, scot, wide, wown, first, second, acc, send_y, recv_y, send_z, recv_z, sums, sums_in,
-    load, store,
+    wout, wnew, fnew, snew,
+    wg, f_all, dirs, x, gcot, scot, wide, wown, first, second, acc, send_y, recv_y, send_z, recv_z, sums, sums_in,
+    load,
     f_send, f_recv, fx_send, fx_recv, fc_send, fc_recv, fd_send, fd_recv,
     ry_send, ry_recv, rz_send, rz_recv, d_send, d_recv, s_send, s_recv, w_send, w_recv,
 ):
@@ -159,8 +159,6 @@
                     w_copies[way, s, h].start()
 
     ring_step(0)
-    own_w = pltpu.make_async_copy(wown, wg.at[me], store.at[0])
-    own_w.start()
 
     for k in [0] + order:
         f_copies[depth + k].wait_recv()
@@ -259,50 +257,70 @@
     whole = sums[...]
     for d in range(1, tp):
         whole = whole + sums_in[d]
-    sums_all[...] = whole
+    gscale = 0.02 / jnp.sqrt(whole[0:1, 0:1] / sizes[0] + 0.25)
+    sscale = 0.02 / jnp.sqrt(whole[1:2, 0:1] / sizes[1] + 0.25)
+    gdir, sdir = both[:, :gc], both[:, gc:]
+
+    def updates(block, at):
+        f = f_all[block, at, :]
+        return (
+            gscale * jnp.dot(f[:, :rank], gdir, preferred_element_type=F32),
+            sscale * jnp.dot(f[:, rank:], sdir, preferred_element_type=F32),
+        )
+
+    def refresh(block, at):
+        gstep, sstep = updates(block, at)
+        wout[block, at, :gc] = (wg[block, at, :gc].astype(F32) - gstep).astype(BF16)
+        wout[block, at, gc:] = (wg[block, at, gc:].astype(F32) - sstep).astype(BF16)
+
+    every = pl.ds(0, rows)
+    gstep, sstep = updates(me, every)
+    wnew[:, :gc] = wide[:, :gc] - gstep
+    wnew[:, gc:] = wide[:, gc:] - sstep
+    wout[me] = wnew[...].astype(BF16)
+    for s in range(1, steps):
+        refresh(at_pos(pos - s), every)
+        refresh(at_pos(pos + s), every)
     for way in (0, 1):
         for h in halves(way, steps - 1):
             w_copies[way, steps - 1, h].wait_recv()
+            refresh(at_pos(pos + steps), pl.ds(h * half, half))
     for group in (w_copies, f_copies, y_copies, z_copies, d_copies):
         for c in group.values():
             c.wait_send()
     for trio in shares.values():
         for c in trio:
             c.wait_send()
-    own_w.wait()
-
-
-def finish_kernel(
-    sizes, wg, f_blk, dirs, sums, gw, sw, gf, sf, fnew, snew,
-    gcopy, scopy, gnew, snew_w, gf_out, gs_out, sf_out, ss_out,
-):
-    gc = gw.shape[1]
-    rank = gf.shape[1]
-    both = dirs[...].reshape(dirs.shape[0] * dirs.shape[1], dirs.shape[2])
-    gdir, sdir = both[:, :gc], both[:, gc:]
-    gscale = 0.02 / jnp.sqrt(sums[0:1, 0:1] / sizes[0] + 0.25)
-    sscale = 0.02 / jnp.sqrt(sums[1:2, 0:1] / sizes[1] + 0.25)
-    w = wg[0]
-    f = f_blk[0]
-    gfull = jnp.dot(f[:, :rank], gdir, preferred_element_type=F32)
-    sfull = jnp.dot(f[:, rank:], sdir, preferred_element_type=F32)
-    gcopy[...] = (w[:, :gc].astype(F32) - gscale * gfull).astype(BF16)
-    scopy[...] = (w[:, gc:].astype(F32) - sscale * sfull).astype(BF16)
-
-    @pl.when(pl.program_id(0) == 0)
-    def _():
-        gnew[...] = gw[...] - gscale * jnp.dot(gf[...], gdir, preferred_element_type=F32)
-        snew_w[...] = sw[...] - sscale * jnp.dot(sf[...], sdir, preferred_element_type=F32)
-        gf_out[...] = fnew[:, :gc]
-        sf_out[...] = fnew[:, gc:]
-        gs_out[...] = snew[:, :gc]
-        ss_out[...] = snew[:, gc:]
+
+
+def finish_kernel(wout, wnew, fnew, snew, gnew, snew_w, gcopy, scopy, gf_out, gs_out, sf_out, ss_out, sems):
+    gc = gnew.shape[1]
+    sc = snew_w.shape[1]
+    n, rows, _ = wout.shape
+    left, right = pl.ds(0, gc), pl.ds(gc, sc)
+    pairs = []
+    for b in range(n):
+        at = pl.ds(b * rows, rows)
+        pairs.append((wout.at[b, :, left], gcopy.at[at, :]))
+        pairs.append((wout.at[b, :, right], scopy.at[at, :]))
+    for src, gate, state in ((wnew, gnew, snew_w), (fnew, gf_out, sf_out), (snew, gs_out, ss_out)):
+        pairs.append((src.at[:, left], gate))
+        pairs.append((src.at[:, right], state))
+    copies = [pltpu.make_async_copy(src, dst, sems.at[k]) for k, (src, dst) in enumerate(pairs)]
+    for c in copies:
+        c.start()
+    for c in copies:
+        c.wait()
 
 
 def per_device(
     n, tp, inputs, gate_cot, state_cot, gate_weight, state_weight, gate_factor, state_factor,
     gate_first, gate_second, state_first, state_second,
 ):
+    args = (
+        inputs, gate_cot, state_cot, gate_weight, state_weight, gate_factor, state_factor,
+        gate_first, gate_second, state_first, state_second,
+    )
     tokens, d = inputs.shape
     rows, gc = gate_weight.shape
     sc = state_weight.shape[1]
@@ -311,22 +329,24 @@
     r = gate_first.shape[0]
     tiles = 3 if tokens % (3 * 128) == 0 else 1
     dma = pltpu.SemaphoreType.DMA
-    anys = pl.BlockSpec(memory_space=pl.ANY)
+    anys = pl.BlockSpec(memory_space=pltpu.HBM)
     sds = jax.ShapeDtypeStruct
     steps = n // 2
-    wg, f_all, dirs, sums, fnew, snew = pl.pallas_call(
-        functools.partial(exchange_kernel, n, tp, tiles),
+    sizes = (n * rows * gc * tp, n * rows * sc * tp)
+    held = pl.pallas_call(
+        functools.partial(exchange_kernel, n, tp, tiles, sizes),
         out_shape=(
-            sds((n, rows, cols), BF16),
-            sds((n, rows, 2 * rank), BF16),
-            sds((n, r, cols), BF16),
-            sds((8, 128), F32),
-            sds((r, cols), F32),
-            sds((r, cols), F32),
+            pltpu.VMEM((n, rows, cols), BF16),
+            pltpu.VMEM((rows, cols), F32),
+            pltpu.VMEM((r, cols), F32),
+            pltpu.VMEM((r, cols), F32),
         ),
         in_specs=[anys] * 11,
-        out_specs=[anys] + [pl.BlockSpec(memory_space=pltpu.VMEM)] * 5,
+        out_specs=[pl.BlockSpec(memory_space=pltpu.VMEM)] * 4,
         scratch_shapes=[
+            pltpu.VMEM((n, rows, cols), BF16),
+            pltpu.VMEM((n, rows, 2 * rank), BF16),
+            pltpu.VMEM((n, r, cols), BF16),
             pltpu.VMEM((tokens, d), BF16),
             pltpu.VMEM((tokens, gc), BF16),
             pltpu.VMEM((tokens, sc), BF16),
@@ -341,7 +361,6 @@
             pltpu.VMEM((8, 128), F32),
             pltpu.VMEM((tp, 8, 128), F32),
             dma((11,)),
-            dma((1,)),
         ]
         + [dma((n,))] * 8
         + [dma((steps,))] * 4
@@ -349,41 +368,23 @@
         + [dma((tp,))] * 2
         + [dma((2, steps, 2))] * 2,
         compiler_params=pltpu.CompilerParams(
-            collective_id=0, has_side_effects=True, vmem_limit_bytes=60 * 1024 * 1024
+            collective_id=0, has_side_effects=True, vmem_limit_bytes=40 * 1024 * 1024
         ),
         name="exchange",
-    )(
-        inputs, gate_cot, state_cot, gate_weight, state_weight, gate_factor, state_factor,
-        gate_first, gate_second, state_first, state_second,
-    )
-
-    def whole(a):
-        return pl.BlockSpec(a.shape, lambda b: (0,) * len(a.shape))
-
-    sizes = (n * rows * gc * tp, n * rows * sc * tp)
-    fixed = (gate_weight, state_weight, gate_factor, state_factor, fnew, snew)
-    outs = (gate_weight, state_weight, gate_first, gate_second, state_first, state_second)
-    gcopy, scopy, gnew, snew_w, *small = pl.pallas_call(
-        functools.partial(finish_kernel, sizes),
-        grid=(n,),
-        out_shape=(sds((n * rows, gc), BF16), sds((n * rows, sc), BF16))
-        + tuple(sds(a.shape, a.dtype) for a in outs),
-        in_specs=[
-            pl.BlockSpec((1, rows, cols), lambda b: (b, 0, 0)),
-            pl.BlockSpec((1, rows, 2 * rank), lambda b: (b, 0, 0)),
-            whole(dirs),
-            whole(sums),
-        ]
-        + [whole(a) for a in fixed],
-        out_specs=[
-            pl.BlockSpec((rows, gc), lambda b: (b, 0)),
-            pl.BlockSpec((rows, sc), lambda b: (b, 0)),
-        ]
-        + [whole(a) for a in outs],
-        compiler_params=pltpu.CompilerParams(vmem_limit_bytes=58 * 1024 * 1024),
+    )(*(pltpu.with_memory_space_constraint(a, pltpu.HBM) for a in args))
+
+    outs = (gate_weight, state_weight, None, None, gate_first, gate_second, state_first, state_second)
+    copies = (sds((n * rows, gc), BF16), sds((n * rows, sc), BF16))
+    shapes = [sds(a.shape, a.dtype) for a in outs[:2]] + list(copies) + [sds(a.shape, a.dtype) for a in outs[4:]]
+    return tuple(pl.pallas_call(
+        finish_kernel,
+        out_shape=tuple(shapes),
+        in_specs=[pl.BlockSpec(memory_space=pltpu.VMEM)] * 4,
+        out_specs=[anys] * 8,
+        scratch_shapes=[dma((2 * n + 6,))],
+        compiler_params=pltpu.CompilerParams(vmem_limit_bytes=4 * 1024 * 1024),
         name="finish",
-    )(wg, f_all, dirs, sums, *fixed)
-    return (gnew, snew_w, gcopy, scopy, *small)
+    )(*(pltpu.with_memory_space_constraint(a, pltpu.VMEM) for a in held)))
 
 
 def lifted_product(inputs, factor, cot):

time: 94.4 us -> 85.5 us (0.906)
  Pallas kernels: 93.4 us -> 84.8 us
    pallas_call x2, Pallas kernels: 93.4 us -> 84.8 us  [the longest x1 81.8 us: per_device(): pl.pallas_call(functools.partial(exchange_kernel, n, tp, tiles, sizes), o...]
where the time goes in v1:
time: 85.5 us; the launch traced here: 85.4 us
  Pallas kernels  84.8 us (99%)
    pallas_call x1, Pallas kernels, per_device(): pl.pallas_call(functools.partial(exchange_kernel, n, tp, tiles, sizes), o...  81.8 us
    pallas_call x1, Pallas kernels, per_device(): pl.pallas_call(finish_kernel, out_shape=tuple(shapes), in_specs=[pl.Block...  3 us

profile of v1, /device:TPU:0, one launch (start us, length us, event | category | flops | bytes accessed | tf_op | source)
XLA Modules:
  0.0 85.4 jit_solution(4409619680026476908)
XLA Ops:
  0.6 81.8 %exchange.1 = (bf16[8,256,1280]{2,1,0:T(8,128)(2,1)S(1)}, f32[256,1280]{1,0:T(8,128)S(1)}, f32[32,1280]{1,0:T(8,128)S(1)}, f32[32,1280]{1,0:T(8,128)S(1)}) custom-call(bf16[1152,2048]{1,0:T(8,128)(2,1)} %x_hbm.1, bf16[1152,1024]{1,0:T(8,128)(2,1)} %gcot_hbm.1, bf16[1152,256]{1,0:T(8,128)(2,1)} %scot_hbm.1, f32[256,1024]{1,0:T(8,128)} %gw_hbm.1, ...), custom_call_target="tpu_custom_call" | custom-call | tf_op jit(solution)/shard_map/exchange/pallas_call | solution.py:336
  82.4 3.0 %finish.1 = (f32[256,1024]{1,0:T(8,128)}, f32[256,256]{1,0:T(8,128)}, bf16[2048,1024]{1,0:T(8,128)(2,1)}, bf16[2048,256]{1,0:T(8,128)(2,1)}, f32[32,1024]{1,0:T(...) custom-call(bf16[8,256,1280]{2,1,0:T(8,128)(2,1)S(1)} %get-tuple-element.12.wout, ...), custom_call_target="tpu_custom_call" | custom-call | tf_op jit(solution)/shard_map/finish/pallas_call | solution.py:379

commit v2 on v1

--- a/solution.py
+++ b/solution.py
@@ -11,6 +11,8 @@
 BF16 = jnp.bfloat16
 F32 = jnp.float32
 
+PLACE = {'a': (0, 1), 'b2': (2,), 'd1': (3, 4), 'd6': (5,), 'e': (6,), 'r1': (7,), 'q0': (8,), 't': (9,), 'u1': (10,), 'u2': (11,), 'u3': (12,), 'v1': (13,), 'w': (14, 15)}
+
 
 def over_rows(a, b):
     return lax.dot_general(a, b, (((0,), (0,)), ((), ())), preferred_element_type=F32)
@@ -25,10 +27,10 @@
     n, tp, tiles, sizes,
     x_hbm, gcot_hbm, scot_hbm, gw_hbm, sw_hbm, gf_hbm, sf_hbm, gfirst_hbm, gsecond_hbm, sfirst_hbm, ssecond_hbm,
     wout, wnew, fnew, snew,
-    wg, f_all, dirs, x, gcot, scot, wide, wown, first, second, acc, send_y, recv_y, send_z, recv_z, sums, sums_in,
+    wg, f_all, dirs, x, gcot, scot, wide, wown, first, second, total, acc, send_y, recv_y, send_z, recv_z, sums, sums_in,
     load,
     f_send, f_recv, fx_send, fx_recv, fc_send, fc_recv, fd_send, fd_recv,
-    ry_send, ry_recv, rz_send, rz_recv, d_send, d_recv, s_send, s_recv, w_send, w_recv,
+    ry_send, ry_recv, rz_send, rz_recv, d_send, d_recv, dy_send, dy_recv, s_send, s_recv, w_send, w_recv,
 ):
     me = lax.axis_index("fs")
     t = lax.axis_index("tp")
@@ -37,7 +39,6 @@
     sc = scot.shape[1]
     r = first.shape[0]
     q = rows // tp
-    half = rows // 2
     depth = n // 2
     z, y = me // 2, me % 2
     partner = 2 * z + 1 - y
@@ -109,6 +110,49 @@
     loads[3].wait()
     wown[...] = wide[...].astype(BF16)
 
+    pos = z + y * (n - 1 - 2 * z)
+
+    def at_pos(p):
+        p = (p + n) % n
+        far = p // (n // 2)
+        return 2 * p * (1 - far) + far * (2 * (n - 1 - p) + 1)
+
+    right, left = at_pos(pos + 1), at_pos(pos - 1)
+    steps = n // 2
+
+    parts = 4
+    piece = rows // parts
+
+    def w_copy(way, s, h):
+        block = at_pos(pos - s) if way == 0 else at_pos(pos + s)
+        at = pl.ds(h * piece, piece)
+        dst = wg.at[block, at, :]
+        src = wown.at[at, :] if s == 0 else dst
+        return remote(
+            src, dst, w_send.at[way, s, h], w_recv.at[way, s, h], (right if way == 0 else left, t)
+        )
+
+    def last_pieces(way):
+        return range(parts // 2) if way == 0 else range(parts // 2, parts)
+
+    w_copies = {}
+
+    def tick(i):
+        s, k = i // parts, i % parts
+        for way in (0, 1):
+            h = k if way == 0 else parts - 1 - k
+            if s > 0:
+                w_copies[way, s - 1, h].wait_recv()
+            if s < steps - 1 or h in last_pieces(way):
+                w_copies[way, s, h] = w_copy(way, s, h)
+                w_copies[way, s, h].start()
+
+    def ticks(name):
+        for i in PLACE.get(name, ()):
+            tick(i)
+
+    ticks('a')
+
     shares = {}
 
     def share(j):
@@ -124,118 +168,166 @@
         f_copies[k].wait_recv()
         pass_over(f_copies, mine, f_send, f_recv, k)
         share(k)
-
-    pos = z + y * (n - 1 - 2 * z)
-
-    def at_pos(p):
-        p = (p + n) % n
-        far = p // (n // 2)
-        return 2 * p * (1 - far) + far * (2 * (n - 1 - p) + 1)
-
-    right, left = at_pos(pos + 1), at_pos(pos - 1)
-    steps = n // 2
-
-    def w_copy(way, s, h):
-        block = at_pos(pos - s) if way == 0 else at_pos(pos + s)
-        dst = wg.at[block, pl.ds(h * half, half), :]
-        src = wown.at[pl.ds(h * half, half), :] if s == 0 else dst
-        return remote(
-            src, dst, w_send.at[way, s, h], w_recv.at[way, s, h], (right if way == 0 else left, t)
-        )
-
-    def halves(way, s):
-        return (0, 1) if s < steps - 1 else (way,)
-
-    w_copies = {}
-
-    def ring_step(s, parts=(0, 1)):
-        for k in parts:
-            for way in (0, 1):
-                h = k if way == 0 else 1 - k
-                if s > 0:
-                    w_copies[way, s - 1, h].wait_recv()
-                if h in halves(way, s):
-                    w_copies[way, s, h] = w_copy(way, s, h)
-                    w_copies[way, s, h].start()
-
-    ring_step(0)
-
-    for k in [0] + order:
+        if k == order[0]:
+            f_copies[depth].wait_recv()
+            share(depth)
+        ticks(f'b{k}')
+
+    for k in order:
         f_copies[depth + k].wait_recv()
         share(depth + k)
+        ticks(f'c{k}')
     for j, pair in shares.items():
         pair[0].wait_recv()
         src = quarter(source_block(j), x_peer)
         cd = remote(src, src, fd_send.at[j], fd_recv.at[j], (me, core_peer))
         cd.start()
         pair.append(cd)
+        ticks(f'd{j}')
     for cx, cc, cd in shares.values():
         cc.wait_recv()
         cd.wait_recv()
 
-    ring_step(1, (0,))
+    ticks('d')
     for k in (4, 5, 6):
         loads[k].wait()
     factor = f_all.reshape(n * rows, 2 * rank)
     step = x.shape[0] // tiles
     acc[...] = jnp.zeros_like(acc)
 
-    def tile(i, carry):
-        at = pl.ds(pl.multiple_of(i * step, step), step)
+    for i in range(tiles):
+        at = pl.ds(i * step, step)
         upper, lower = split(jnp.dot(x[at, :], factor[...], preferred_element_type=F32))
         g, s = gcot[at, :], scot[at, :]
         acc[:, :gc] += over_rows(upper[:, :rank], g) + over_rows(lower[:, :rank], g)
         acc[:, gc:] += over_rows(upper[:, rank:], s) + over_rows(lower[:, rank:], s)
-        return carry
-
-    lax.fori_loop(0, tiles, tile, 0)
+        ticks(f'm{i}')
 
     def part_of(block):
         return acc[pl.ds(pl.multiple_of(block * r, r), r), :]
 
-    out_order = list(range(1, depth)) + [0]
+    low = z < depth // 2
+    flip = 1 - low.astype(jnp.int32)
+    zz = z + flip * (depth - 1 - 2 * z)
+    ahead = z + 1 - 2 * flip
+    behind = z - 1 + 2 * flip
+
+    def level(k):
+        return k + flip * (depth - 1 - 2 * k)
+
     y_copies = {}
-    for k in out_order:
-        send_y[k] = part_of(2 * ((z + k) % depth) + 1 - y).astype(BF16)
+    for k in reversed(range(depth)):
+        send_y[k] = part_of(2 * level(k) + 1 - y).astype(BF16)
         y_copies[k] = remote(send_y.at[k], recv_y.at[k], ry_send.at[k], ry_recv.at[k], (partner, t))
         y_copies[k].start()
-    ring_step(1, (1,))
+    ticks('e')
 
     grams = []
     for k in (0, 1):
         part = factor[:, k * rank:(k + 1) * rank]
         grams.append(split(over_rows(part, part)))
 
-    z_copies = {}
-    for k in range(1, depth):
+    ticks('g')
+    def hop(way, k, target):
+        goal = level(k)
+        return remote(
+            send_z.at[goal], recv_z.at[way, goal], rz_send.at[goal], rz_recv.at[way, goal],
+            (2 * target + y, t),
+        )
+
+    def add_on(total, way, k):
+        hop(way, k, z).wait_recv()
+        return total + recv_z[way, level(k)].astype(F32)
+
+    def both_rows(k):
         y_copies[k].wait_recv()
-        send_z[k] = (part_of(along_z(k)) + recv_y[k].astype(F32)).astype(BF16)
-        z_copies[k] = remote(send_z.at[k], recv_z.at[k], rz_send.at[k], rz_recv.at[k], (along_z(k), t))
-        z_copies[k].start()
-
-    ring_step(2, (0,))
+        return part_of(2 * level(k) + y) + recv_y[k].astype(F32)
+
+    def pass_up(k):
+        @pl.when(zz > 0)
+        def _():
+            send_z[level(k)] = add_on(both_rows(k), flip, k).astype(BF16)
+
+        @pl.when(zz == 0)
+        def _():
+            send_z[level(k)] = both_rows(k).astype(BF16)
+
+        hop(flip, k, ahead).start()
+
+    for k in reversed(range(1, depth)):
+        pl.when(zz < k)(functools.partial(pass_up, k))
+        ticks(f'r{k}')
+    for k in range(depth // 2 - 1):
+        @pl.when(zz > k)
+        def _():
+            send_z[level(k)] = add_on(both_rows(k), 1 - flip, k).astype(BF16)
+            hop(1 - flip, k, behind).start()
+        ticks(f'q{k}')
+
+    ticks('s')
 
     for c in loads[7:]:
         c.wait()
-    y_copies[0].wait_recv()
-    total = part_of(me) + recv_y[0].astype(F32)
-    for k in range(1, depth):
-        z_copies[k].wait_recv()
-        total = total + recv_z[k].astype(F32)
-    new_first = 0.8 * first[...] + 0.2 * total
-    new_second = 0.9 * second[...] + 0.1 * total * total
+    for k in range(depth // 2):
+        @pl.when(zz == k)
+        def _():
+            total[...] = add_on(both_rows(k), 1 - flip, k)
+            if k > 0:
+                total[...] = add_on(total[...], flip, k)
+
+    proj = total[...]
+    new_first = 0.8 * first[...] + 0.2 * proj
+    new_second = 0.9 * second[...] + 0.1 * proj * proj
     fnew[...] = new_first
     snew[...] = new_second
     dirs[me] = (new_first / jnp.sqrt(new_second)).astype(BF16)
-    view = lambda b: dirs.at[b]
-    d_copies = first_leg(view, d_send, d_recv)
-    for k in order:
-        d_copies[k].wait_recv()
-        pass_over(d_copies, view, d_send, d_recv, k)
-
-    ring_step(2, (1,))
-    for k in range(depth):
-        d_copies[depth + k].wait_recv()
+    def d_hop(way, j):
+        origin = z + 1 - j if way == 0 else z - 1 + j
+        view = dirs.at[2 * origin + y]
+        target = z + 1 if way == 0 else z - 1
+        return remote(view, view, d_send.at[way, j], d_recv.at[way, j], (2 * target + y, t))
+
+    def d_in(way, j):
+        origin = z - j if way == 0 else z + j
+        view = dirs.at[2 * origin + y]
+        return remote(view, view, d_send.at[way, j], d_recv.at[way, j], (me, t))
+
+    def d_over(way, j):
+        origin = z - j if way == 0 else z + j
+        view = dirs.at[2 * origin + y]
+        return remote(view, view, dy_send.at[way, j], dy_recv.at[way, j], (partner, t))
+
+    def d_over_in(way, j):
+        origin = z - j if way == 0 else z + j
+        view = dirs.at[2 * origin + 1 - y]
+        return remote(view, view, dy_send.at[way, j], dy_recv.at[way, j], (partner, t))
+
+    def there(way, j):
+        return z >= j if way == 0 else z < depth - j
+
+    def more(way):
+        return there(1 - way, 1)
+
+    for way in (0, 1):
+        pl.when(more(way))(d_hop(way, 1).start)
+    d_over(0, 0).start()
+    ticks('t')
+    for j in range(1, depth):
+        for way in (0, 1):
+            @pl.when(there(way, j))
+            def _():
+                d_in(way, j).wait_recv()
+                if j < depth - 1:
+                    pl.when(more(way))(d_hop(way, j + 1).start)
+                d_over(way, j).start()
+        ticks(f'u{j}')
+
+    ticks('v')
+    d_over_in(0, 0).wait_recv()
+    for j in range(1, depth):
+        for way in (0, 1):
+            pl.when(there(way, j))(d_over_in(way, j).wait_recv)
+        ticks(f'v{j}')
     both = dirs[...].reshape(n * r, dirs.shape[2])
     squares = []
     for (upper, lower), part in zip(grams, (both[:, :gc], both[:, gc:])):
@@ -250,8 +342,7 @@
         c.start()
         s_copies.append(c)
 
-    for s in range(3, steps):
-        ring_step(s)
+    ticks('w')
     for c in s_copies:
         c.wait()
     whole = sums[...]
@@ -281,13 +372,26 @@
     for s in range(1, steps):
         refresh(at_pos(pos - s), every)
         refresh(at_pos(pos + s), every)
+    ticks('x')
     for way in (0, 1):
-        for h in halves(way, steps - 1):
+        for h in last_pieces(way):
             w_copies[way, steps - 1, h].wait_recv()
-            refresh(at_pos(pos + steps), pl.ds(h * half, half))
-    for group in (w_copies, f_copies, y_copies, z_copies, d_copies):
+        at = pl.ds(way * (rows // 2), rows // 2)
+        refresh(at_pos(pos + steps), at)
+    for c in w_copies.values():
+        c.wait_send()
+    for group in (f_copies, y_copies):
         for c in group.values():
             c.wait_send()
+    for k in range(1, depth):
+        pl.when(zz < k)(hop(flip, k, ahead).wait_send)
+    for k in range(depth // 2 - 1):
+        pl.when(zz > k)(hop(1 - flip, k, behind).wait_send)
+    d_over(0, 0).wait_send()
+    for way in (0, 1):
+        for j in range(1, depth):
+            pl.when(more(way) & there(way, j - 1))(d_hop(way, j).wait_send)
+            pl.when(there(way, j))(d_over(way, j).wait_send)
     for trio in shares.values():
         for c in trio:
             c.wait_send()
@@ -354,19 +458,21 @@
             pltpu.VMEM((rows, cols), BF16),
             pltpu.VMEM((r, cols), F32),
             pltpu.VMEM((r, cols), F32),
+            pltpu.VMEM((r, cols), F32),
             pltpu.VMEM((rank, cols), F32),
         ]
-        + [pltpu.VMEM((steps, r, cols), BF16)] * 4
+        + [pltpu.VMEM((steps, r, cols), BF16)] * 3
+        + [pltpu.VMEM((2, steps, r, cols), BF16)]
         + [
             pltpu.VMEM((8, 128), F32),
             pltpu.VMEM((tp, 8, 128), F32),
             dma((11,)),
         ]
         + [dma((n,))] * 8
-        + [dma((steps,))] * 4
-        + [dma((n,))] * 2
+        + [dma((steps,))] * 3
+        + [dma((2, steps))] * 5
         + [dma((tp,))] * 2
-        + [dma((2, steps, 2))] * 2,
+        + [dma((2, steps, 4))] * 2,
         compiler_params=pltpu.CompilerParams(
             collective_id=0, has_side_effects=True, vmem_limit_bytes=40 * 1024 * 1024
         ),

time: 85.5 us -> 82.1 us (0.960)
  Pallas kernels: 84.8 us -> 81.3 us
    pallas_call x1, Pallas kernels: 81.8 us -> 78.3 us  [per_device(): pl.pallas_call(functools.partial(exchange_kernel, n, tp, tiles, sizes), o...]
where the time goes in v2:
time: 82.1 us; the launch traced here: 82 us
  Pallas kernels  81.3 us (99%)
    pallas_call x1, Pallas kernels, per_device(): pl.pallas_call(functools.partial(exchange_kernel, n, tp, tiles, sizes), o...  78.3 us
    pallas_call x1, Pallas kernels, per_device(): pl.pallas_call(finish_kernel, out_shape=tuple(shapes), in_specs=[pl.Block...  3 us

profile of v2, /device:TPU:0, one launch (start us, length us, event | category | flops | bytes accessed | tf_op | source)
XLA Modules:
  0.0 82.0 jit_solution(12195294537408524894)
XLA Ops:
  0.6 78.3 %exchange.1 = (bf16[8,256,1280]{2,1,0:T(8,128)(2,1)S(1)}, f32[256,1280]{1,0:T(8,128)S(1)}, f32[32,1280]{1,0:T(8,128)S(1)}, f32[32,1280]{1,0:T(8,128)S(1)}) custom-call(bf16[1152,2048]{1,0:T(8,128)(2,1)} %x_hbm.1, bf16[1152,1024]{1,0:T(8,128)(2,1)} %gcot_hbm.1, bf16[1152,256]{1,0:T(8,128)(2,1)} %scot_hbm.1, f32[256,1024]{1,0:T(8,128)} %gw_hbm.1, ...), custom_call_target="tpu_custom_call" | custom-call | tf_op jit(solution)/shard_map/exchange/pallas_call | solution.py:440
  79.0 3.0 %finish.1 = (f32[256,1024]{1,0:T(8,128)}, f32[256,256]{1,0:T(8,128)}, bf16[2048,1024]{1,0:T(8,128)(2,1)}, bf16[2048,256]{1,0:T(8,128)(2,1)}, f32[32,1024]{1,0:T(...) custom-call(bf16[8,256,1280]{2,1,0:T(8,128)(2,1)S(1)} %get-tuple-element.12.wout, ...), custom_call_target="tpu_custom_call" | custom-call | tf_op jit(solution)/shard_map/finish/pallas_call | solution.py:485

commit v3 on v2

--- a/solution.py
+++ b/solution.py
@@ -11,7 +11,8 @@
 BF16 = jnp.bfloat16
 F32 = jnp.float32
 
-PLACE = {'a': (0, 1), 'b2': (2,), 'd1': (3, 4), 'd6': (5,), 'e': (6,), 'r1': (7,), 'q0': (8,), 't': (9,), 'u1': (10,), 'u2': (11,), 'u3': (12,), 'v1': (13,), 'w': (14, 15)}
+KINDS = "omiy"
+PLACE = {'a': ((0, 'omiy'), (1, 'miy'), (2, 'mi'), (3, 'mi')), 'c1': ((2, 'y'), (3, 'y'), (4, 'y'), (5, 'm')), 'd1': ((5, 'y'), (6, 'm')), 'r2': ((6, 'y'), (7, 'y'), (8, 'y'), (9, 'y')), 'r1': ((8, 'm'), (10, 'y')), 'v': ((11, 'y'),), 'v2': ((12, 'y'), (13, 'o'), (14, 'i')), 'w': ((13, 'my'), (14, 'omy'), (15, 'omy')), 'b3': ((1, 'o'), (2, 'o'), (3, 'o'), (4, 'm')), 'c2': ((4, 'o'), (5, 'o')), 'd3': ((6, 'o'),), 'q0': ((7, 'o'), (8, 'o')), 't': ((9, 'om'), (10, 'o'), (11, 'o'), (12, 'o')), 'b2': ((4, 'i'),), 'd5': ((5, 'i'),), 'd': ((6, 'i'),), 'g': ((7, 'i'), (8, 'i'), (9, 'i')), 's': ((10, 'i'),), 'u1': ((10, 'm'), (11, 'i')), 'u3': ((11, 'm'), (12, 'i'), (13, 'i')), 'v3': ((15, 'i'),), 'm0': ((7, 'm'),), 'v1': ((12, 'm'),)}
 
 
 def over_rows(a, b):
@@ -132,24 +133,43 @@
             src, dst, w_send.at[way, s, h], w_recv.at[way, s, h], (right if way == 0 else left, t)
         )
 
-    def last_pieces(way):
-        return range(parts // 2) if way == 0 else range(parts // 2, parts)
+    def in_first(p, h):
+        p = (p + n) % n % steps
+        share = parts // 2 - (p == 0).astype(jnp.int32) + (p == steps - 1).astype(jnp.int32)
+        return h < share
+
+    def sent(way, s, h):
+        if s < steps - 1:
+            return pos >= 0
+        return in_first(pos + 1, h) if way == 0 else ~in_first(pos - 1, h)
 
     w_copies = {}
 
-    def tick(i):
-        s, k = i // parts, i % parts
-        for way in (0, 1):
-            h = k if way == 0 else parts - 1 - k
-            if s > 0:
-                w_copies[way, s - 1, h].wait_recv()
-            if s < steps - 1 or h in last_pieces(way):
-                w_copies[way, s, h] = w_copy(way, s, h)
-                w_copies[way, s, h].start()
+    spot = pos % steps
+
+    def forward(way, s, k):
+        h = k if way == 0 else parts - 1 - k
+        if s > 0:
+            w_copies[way, s - 1, h].wait_recv()
+        if s < steps - 1:
+            w_copies[way, s, h].start()
+        elif k < parts - 1:
+            pl.when(sent(way, s, h))(w_copies[way, s, h].start)
 
     def ticks(name):
-        for i in PLACE.get(name, ()):
-            tick(i)
+        for i, kinds in PLACE.get(name, ()):
+            s, k = i // parts, i % parts
+            for way in (0, 1):
+                h = k if way == 0 else parts - 1 - k
+                if s < steps - 1 or k < parts - 1:
+                    w_copies[way, s, h] = w_copy(way, s, h)
+                if len(kinds) == len(KINDS):
+                    forward(way, s, k)
+                    continue
+                for kind in kinds:
+                    at = KINDS.index(kind)
+                    at = at if way == 0 else steps - 1 - at
+                    pl.when(spot == at)(functools.partial(forward, way, s, k))
 
     ticks('a')
 
@@ -373,13 +393,15 @@
         refresh(at_pos(pos - s), every)
         refresh(at_pos(pos + s), every)
     ticks('x')
-    for way in (0, 1):
-        for h in last_pieces(way):
-            w_copies[way, steps - 1, h].wait_recv()
-        at = pl.ds(way * (rows // 2), rows // 2)
-        refresh(at_pos(pos + steps), at)
-    for c in w_copies.values():
-        c.wait_send()
+    for h in range(parts):
+        first_way = in_first(pos, h)
+        if h < parts - 1:
+            pl.when(first_way)(w_copies[0, steps - 1, h].wait_recv)
+        if h > 0:
+            pl.when(~first_way)(w_copies[1, steps - 1, h].wait_recv)
+    refresh(at_pos(pos + steps), every)
+    for (way, s, h), c in w_copies.items():
+        pl.when(sent(way, s, h))(c.wait_send)
     for group in (f_copies, y_copies):
         for c in group.values():
             c.wait_send()

time: 82.1 us -> 78.4 us (0.955)
  Pallas kernels: 81.3 us -> 77.6 us
    pallas_call x1, Pallas kernels: 78.3 us -> 74.6 us  [per_device(): pl.pallas_call(functools.partial(exchange_kernel, n, tp, tiles, sizes), o...]
where the time goes in v3:
time: 78.4 us; the launch traced here: 78.3 us
  Pallas kernels  77.6 us (99%)
    pallas_call x1, Pallas kernels, per_device(): pl.pallas_call(functools.partial(exchange_kernel, n, tp, tiles, sizes), o...  74.6 us
    pallas_call x1, Pallas kernels, per_device(): pl.pallas_call(finish_kernel, out_shape=tuple(shapes), in_specs=[pl.Block...  3 us

profile of v3, /device:TPU:0, one launch (start us, length us, event | category | flops | bytes accessed | tf_op | source)
XLA Modules:
  0.0 78.3 jit_solution(8757540440836429815)
XLA Ops:
  0.6 74.6 %exchange.1 = (bf16[8,256,1280]{2,1,0:T(8,128)(2,1)S(1)}, f32[256,1280]{1,0:T(8,128)S(1)}, f32[32,1280]{1,0:T(8,128)S(1)}, f32[32,1280]{1,0:T(8,128)S(1)}) custom-call(bf16[1152,2048]{1,0:T(8,128)(2,1)} %x_hbm.1, bf16[1152,1024]{1,0:T(8,128)(2,1)} %gcot_hbm.1, bf16[1152,256]{1,0:T(8,128)(2,1)} %scot_hbm.1, f32[256,1024]{1,0:T(8,128)} %gw_hbm.1, ...), custom_call_target="tpu_custom_call" | custom-call | tf_op jit(solution)/shard_map/exchange/pallas_call | solution.py:462
  75.3 3.0 %finish.1 = (f32[256,1024]{1,0:T(8,128)}, f32[256,256]{1,0:T(8,128)}, bf16[2048,1024]{1,0:T(8,128)(2,1)}, bf16[2048,256]{1,0:T(8,128)(2,1)}, f32[32,1024]{1,0:T(...) custom-call(bf16[8,256,1280]{2,1,0:T(8,128)(2,1)S(1)} %get-tuple-element.12.wout, ...), custom_call_target="tpu_custom_call" | custom-call | tf_op jit(solution)/shard_map/finish/pallas_call | solution.py:507

commit v4 on v3

--- a/solution.py
+++ b/solution.py
@@ -399,7 +399,8 @@
             pl.when(first_way)(w_copies[0, steps - 1, h].wait_recv)
         if h > 0:
             pl.when(~first_way)(w_copies[1, steps - 1, h].wait_recv)
-    refresh(at_pos(pos + steps), every)
+        if h % 2 == 1:
+            refresh(at_pos(pos + steps), pl.ds((h - 1) * piece, 2 * piece))
     for (way, s, h), c in w_copies.items():
         pl.when(sent(way, s, h))(c.wait_send)
     for group in (f_copies, y_copies):

time: 78.4 us -> 78.6 us (level)
  no operation moved by 1% of the time
where the time goes in v4:
time: 78.6 us; the launch traced here: 78.4 us
  Pallas kernels  77.8 us (99%)
    pallas_call x1, Pallas kernels, per_device(): pl.pallas_call(functools.partial(exchange_kernel, n, tp, tiles, sizes), o...  74.8 us
    pallas_call x1, Pallas kernels, per_device(): pl.pallas_call(finish_kernel, out_shape=tuple(shapes), in_specs=[pl.Block...  3 us

profile of v4, /device:TPU:0, one launch (start us, length us, event | category | flops | bytes accessed | tf_op | source)
XLA Modules:
  0.0 78.4 jit_solution(18041943495501074622)
XLA Ops:
  0.6 74.8 %exchange.1 = (bf16[8,256,1280]{2,1,0:T(8,128)(2,1)S(1)}, f32[256,1280]{1,0:T(8,128)S(1)}, f32[32,1280]{1,0:T(8,128)S(1)}, f32[32,1280]{1,0:T(8,128)S(1)}) custom-call(bf16[1152,2048]{1,0:T(8,128)(2,1)} %x_hbm.1, bf16[1152,1024]{1,0:T(8,128)(2,1)} %gcot_hbm.1, bf16[1152,256]{1,0:T(8,128)(2,1)} %scot_hbm.1, f32[256,1024]{1,0:T(8,128)} %gw_hbm.1, ...), custom_call_target="tpu_custom_call" | custom-call | tf_op jit(solution)/shard_map/exchange/pallas_call | solution.py:463
  75.4 3.0 %finish.1 = (f32[256,1024]{1,0:T(8,128)}, f32[256,256]{1,0:T(8,128)}, bf16[2048,1024]{1,0:T(8,128)(2,1)}, bf16[2048,256]{1,0:T(8,128)(2,1)}, f32[32,1024]{1,0:T(...) custom-call(bf16[8,256,1280]{2,1,0:T(8,128)(2,1)S(1)} %get-tuple-element.12.wout, ...), custom_call_target="tpu_custom_call" | custom-call | tf_op jit(solution)/shard_map/finish/pallas_call | solution.py:508
